TPU v7x, 32 devices: a whole 2x2x4 slice. The times are simulated.
32 devices in a mesh: sp: 8 (over z, x), tp: 4 (over y, core).
Axes of the slice: x: 2, y: 2, z: 4, core: 2. Of those that a mesh axis runs over, the one named last changes fastest.
Arguments:
- residual: bfloat16 [1024, 2048], P(('sp', 'tp')), may hold values from -6 to 6
- query_first: bfloat16 [1024, 1024], P('sp', 'tp'), may hold values from -200 to 200
- key_first: bfloat16 [1024, 1024], P('sp', 'tp'), may hold values from -200 to 200
- query_second: bfloat16 [1024, 1024], P('sp', 'tp'), may hold values from -200 to 200
- key_second: bfloat16 [1024, 1024], P('sp', 'tp'), may hold values from -200 to 200
- values: bfloat16 [1024, 2048], P('sp', 'tp'), may hold values from -6 to 6
- lambda_weight: float32 [16], P('tp'), may hold values from 0.3 to 0.8
- head_gain: float32 [128], replicated, may hold values from 0.1 to 1.9
- out_weight: bfloat16 [2048, 2048], P('sp', 'tp'), may hold values from -0.125 to 0.125
- norm_gain: float32 [2048], replicated, may hold values from 0.1 to 1.9
- gate_weight: bfloat16 [2048, 5632], P(None, 'tp'), may hold values from -0.125 to 0.125
- up_weight: bfloat16 [2048, 5632], P(None, 'tp'), may hold values from -0.125 to 0.125
- down_weight: bfloat16 [2048, 5632], P('sp', 'tp'), may hold values from -0.078125 to 0.078125
Outputs:
- layer_out: bfloat16 [1024, 2048], P(('sp', 'tp'))
All inputs are finite; a program needn't handle non-finite values.
Results may differ from a plain program's by a relative error of at most 0.017.
Values may be sent and summed in bfloat16 or wider, within the bound.
A program may use at most 128 MiB of HBM per device.

v0:
```python
import math

import jax
import jax.numpy as jnp
from jax import lax
from jax.sharding import PartitionSpec as P

epsilon = 1e-06


def map_update(state_in, queries, key_rows, value_block, score_scale):
    maxima, totals, accumulated = state_in
    scores = (
        jnp.einsum("thd,khd->htk", queries, key_rows, preferred_element_type=jnp.float32)
        * score_scale
    )
    newest = jnp.maximum(maxima, jnp.max(scores, axis=-1))
    factor = jnp.exp(maxima - newest)
    weights = jnp.exp(scores - newest[:, :, None])
    totals = totals * factor + jnp.sum(weights, axis=-1)
    product = jnp.einsum(
        "htk,khe->the",
        weights.astype(jnp.bfloat16),
        value_block,
        preferred_element_type=jnp.float32,
    )
    accumulated = accumulated * factor.T[:, :, None] + product
    return (newest, totals, accumulated)


def local(
    residual,
    query_first,
    key_first,
    query_second,
    key_second,
    values,
    lambda_weight,
    head_gain,
    out_weight,
    norm_gain,
    gate_weight,
    up_weight,
    down_weight,
):
    tokens_here = query_first.shape[0]
    head_count = lambda_weight.shape[0]
    head_size = query_first.shape[1] // head_count
    value_size = values.shape[1] // head_count
    score_scale = head_size ** (-0.5)
    queries_first = query_first.reshape(tokens_here, head_count, head_size)
    queries_second = query_second.reshape(tokens_here, head_count, head_size)
    empty_stats = (
        jnp.full((head_count, tokens_here), -jnp.inf, jnp.float32),
        jnp.zeros((head_count, tokens_here), jnp.float32),
        jnp.zeros((tokens_here, head_count, value_size), jnp.float32),
    )
    start_state = (empty_stats, empty_stats)
    keys_one = lax.all_gather(key_first, "sp", axis=0, tiled=True)
    row_count = keys_one.shape[0]
    block_rows = math.gcd(row_count, 1024)
    blocks = (
        keys_one.reshape(row_count // block_rows, block_rows, head_count, head_size),
        lax.all_gather(key_second, "sp", axis=0, tiled=True).reshape(
            row_count // block_rows, block_rows, head_count, head_size
        ),
        lax.all_gather(values, "sp", axis=0, tiled=True).reshape(
            row_count // block_rows, block_rows, head_count, value_size
        ),
    )

    def advance(current, block_keys):
        return (
            (
                map_update(current[0], queries_first, block_keys[0], block_keys[2], score_scale),
                map_update(current[1], queries_second, block_keys[1], block_keys[2], score_scale),
            ),
            None,
        )

    statistics = lax.scan(advance, start_state, blocks)[0]

    def finish(map_stats):
        return map_stats[2] / map_stats[1].T[:, :, None]

    difference = finish(statistics[0]) - lambda_weight[None, :, None] * finish(statistics[1])
    scaled = difference * lax.rsqrt(
        jnp.mean(difference * difference, axis=-1, keepdims=True) + epsilon
    )
    attended = (
        (scaled * head_gain).astype(jnp.bfloat16).reshape(tokens_here, head_count * value_size)
    )
    partial_value = lax.dot_general(
        attended,
        lax.all_gather(out_weight, "sp", axis=0, tiled=True),
        (((1,), (1,)), ((), ())),
        preferred_element_type=jnp.float32,
    )
    summed = lax.psum_scatter(
        partial_value.astype(jnp.bfloat16), "tp", scatter_dimension=0, tiled=True
    ).astype(jnp.float32)
    after_attention = (residual.astype(jnp.float32) + summed).astype(jnp.bfloat16)
    stream = after_attention.astype(jnp.float32)
    scaled_rows = stream * lax.rsqrt(jnp.mean(stream * stream, axis=-1, keepdims=True) + epsilon)
    shard_piece = lax.all_gather(
        (scaled_rows * norm_gain).astype(jnp.bfloat16), "tp", axis=0, tiled=True
    )
    gate_part = jnp.dot(shard_piece, gate_weight, preferred_element_type=jnp.float32)
    up_part = jnp.dot(shard_piece, up_weight, preferred_element_type=jnp.float32)
    hidden = (jax.nn.silu(gate_part) * up_part).astype(jnp.bfloat16)
    down_partial = lax.dot_general(
        hidden,
        lax.all_gather(down_weight, "sp", axis=0, tiled=True),
        (((1,), (1,)), ((), ())),
        preferred_element_type=jnp.float32,
    )
    feed_out = lax.psum_scatter(
        down_partial.astype(jnp.bfloat16), "tp", scatter_dimension=0, tiled=True
    ).astype(jnp.float32)
    return (after_attention.astype(jnp.float32) + feed_out).astype(jnp.bfloat16)


def solution(mesh):
    return jax.shard_map(
        local,
        mesh=mesh,
        in_specs=(
            P(("sp", "tp"), None),
            P("sp", "tp"),
            P("sp", "tp"),
            P("sp", "tp"),
            P("sp", "tp"),
            P("sp", "tp"),
            P("tp"),
            P(),
            P("sp", "tp"),
            P(),
            P(None, "tp"),
            P(None, "tp"),
            P("sp", "tp"),
        ),
        out_specs=P(("sp", "tp"), None),
        check_vma=False,
    )
```

profile of v0, /device:TPU:0, one launch (start us, length us, event | category | flops | bytes accessed | tf_op | source)
XLA Modules:
  0.0 259.6 jit_solution(6984431258322703495)
XLA Ops:
  6.5 0.7 all-gather.4.cloned.1.call-update
  7.3 0.7 all-gather.6.cloned.1.call-update
  8.1 33.7 %all_gather.18 = bf16[1024,256]{1,0:T(8,128)(2,1)S(1)} all-gather(bf16[128,256]{1,0:T(8,128)(2,1)} %param.15), channel_id=1, replica_groups=mesh['sp'=8,'tp'=4] {'sp'}, dimensions={0}, use_global_device_ids=true | all-gather | bytes 589824 | tf_op jit(solution)/shard_map/all_gather | solution.py:59
  42.0 1.0 copy.19
  43.0 32.2 %all_gather.20 = bf16[1024,256]{1,0:T(8,128)(2,1)S(1)} all-gather(bf16[128,256]{1,0:T(8,128)(2,1)S(1)} %copy-done.4), channel_id=1, replica_groups=mesh['sp'=8,'tp'=4] {'sp'}, dimensions={0}, use_global_device_ids=true | all-gather | bytes 589824 | tf_op jit(solution)/shard_map/all_gather | solution.py:64
  75.5 0.6 multiply_reduce_fusion.1
  76.5 0.6 multiply_reduce_fusion
  77.1 1.3 copy-done
  79.0 1.5 copy.21
  80.5 0.7 fusion.10
  81.2 0.9 copy-done.1
  82.1 0.7 multiply_reduce_fusion.2
  82.9 22.5 %all-gather.6.cloned.1.call-done = bf16[2048,512]{1,0:T(8,128)(2,1)} async-done(((bf16[256,512]{1,0:T(8,128)(2,1)}), bf16[2048,512]{1,0:T(8,128)(2,1)}) %all-gather.6.cloned.1.call-update) | async-done | bytes 2097168 | tf_op jit(solution)/shard_map/all_gather | solution.py:95
  105.5 3.2 %convolution_convert_fusion = bf16[128,2048]{1,0:T(8,128)(2,1)} fusion(bf16[128,512]{0,1:T(8,128)(2,1)S(1)} %bitcast.51, bf16[2048,512]{1,0:T(8,128)(2,1)} %all-gather.6.cloned.1.call-done), kind=kOutput, calls=%fused_computation.2 | convolution fusion | flops 268697600 | bytes 2752512 | tf_op jit(solution)/shard_map/dot_general | solution.py:93
  108.7 0.5 all-gather.8.cloned.1.call-update
  109.3 19.8 %reduce-scatter.3.cloned.1.call-done = bf16[32,2048]{1,0:T(8,128)(2,1)} async-done(((bf16[128,2048]{1,0:T(8,128)(2,1)}), bf16[32,2048]{1,0:T(8,128)(2,1)}) %reduce-scatter.3.cloned.1.call-update) | async-done | bytes 131088 | tf_op jit(solution)/shard_map/reduce_scatter | solution.py:99
  129.1 1.1 fusion.18
  130.2 1.0 fusion.20
  131.2 6.6 %all_gather.22 = bf16[128,2048]{1,0:T(8,128)(2,1)S(1)} all-gather(bf16[32,2048]{1,0:T(8,128)(2,1)S(1)} %fusion.20), channel_id=1, replica_groups=mesh['sp'=8,'tp'=4] {'tp'}, dimensions={0}, use_global_device_ids=true | all-gather | bytes 655360 | tf_op jit(solution)/shard_map/all_gather | solution.py:105
  137.8 4.0 %fusion.25 = f32[128,1408]{1,0:T(8,128)S(1)} fusion(bf16[128,2048]{1,0:T(8,128)(2,1)S(1)} %all_gather.22, bf16[2048,1408]{1,0:T(8,128)(2,1)} %param.23), kind=kOutput, calls=%fused_computation.44 | convolution fusion | flops 738197504 | bytes 7012352 | tf_op jit(solution)/shard_map/dot_general | solution.py:108
  141.8 81.6 %all-gather.8.cloned.1.call-done = bf16[2048,1408]{1,0:T(8,128)(2,1)} async-done(((bf16[256,1408]{1,0:T(8,128)(2,1)}), bf16[2048,1408]{1,0:T(8,128)(2,1)}) %all-gather.8.cloned.1.call-update) | async-done | bytes 5767184 | tf_op jit(solution)/shard_map/all_gather | solution.py:113
  223.5 8.0 %convolution_convert_fusion.1 = bf16[128,2048]{1,0:T(8,128)(2,1)} fusion(bf16[2048,1408]{1,0:T(8,128)(2,1)} %all-gather.8.cloned.1.call-done, bf16[128,2048]{1,0:T(8,128)(2,1)S(1)} %all_gather.22, bf16[2048,1408]{1,0:T(8,128)(2,1)} %param.24, f32[128,1408]{1,0:T(8,128)S(1)} %fusion.25), kind=kOutput, calls=%fused_computation.3 | convolution fusion | flops 1477738496 | bytes 13303808 | tf_op jit(solution)/shard_map/dot_general | solution.py:111
  231.5 20.0 %reduce-scatter.5.cloned.1.call-done = bf16[32,2048]{1,0:T(8,128)(2,1)} async-done(((bf16[128,2048]{1,0:T(8,128)(2,1)}), bf16[32,2048]{1,0:T(8,128)(2,1)}) %reduce-scatter.5.cloned.1.call-update) | async-done | bytes 131088 | tf_op jit(solution)/shard_map/reduce_scatter | solution.py:117
  251.5 1.6 fusion.21
  (36 shorter events, 1.9 us)
Async XLA Ops:
  6.5 36.4 %copy-start.4 = (bf16[128,256]{1,0:T(8,128)(2,1)S(1)}, bf16[128,256]{1,0:T(8,128)(2,1)}, u32[]{:S(2)}) copy-start(bf16[128,256]{1,0:T(8,128)(2,1)} %param.17) | copy-start | bytes 196612
  6.5 68.8 %copy-start.5 = (bf16[128,256]{1,0:T(8,128)(2,1)S(1)}, bf16[128,256]{1,0:T(8,128)(2,1)}, u32[]{:S(2)}) copy-start(bf16[128,256]{1,0:T(8,128)(2,1)} %param.16) | copy-start | bytes 196612
  6.5 72.5 %all-gather.4.cloned.1.call-start = ((), (), s32[]{:S(2)}) async-start(), calls=%async_computation.2 | async-start | bytes 1179648 | tf_op jit(solution)/shard_map/all_gather | solution.py:67
  7.3 98.2 %all-gather.6.cloned.1.call-start = ((), (), s32[]{:S(2)}) async-start(), calls=%async_computation.3 | async-start | bytes 2359296 | tf_op jit(solution)/shard_map/all_gather | solution.py:95
  8.0 121.1 %reduce-scatter.3.cloned.1.call-start = ((), (), s32[]{:S(2)}) async-start(), calls=%async_computation.4 | async-start | bytes 655360 | tf_op jit(solution)/shard_map/reduce_scatter | solution.py:99
  77.1 1.3 copy-start
  80.5 1.6 copy-start.1
  80.5 1.6 copy-start.8
  82.1 0.7 copy-start.7
  82.9 46.2 %copy-start.2 = (bf16[32,2048]{1,0:T(8,128)(2,1)S(1)}, bf16[32,2048]{1,0:T(8,128)(2,1)}, u32[]{:S(2)}) copy-start(bf16[32,2048]{1,0:T(8,128)(2,1)} %param.13) | copy-start | bytes 393220
  105.5 24.7 %copy-start.6 = (f32[2048]{0:T(1024)S(1)}, f32[2048]{0:T(1024)}, u32[]{:S(2)}) copy-start(f32[2048]{0:T(1024)} %param.22) | copy-start | bytes 24580
  108.7 114.8 %all-gather.8.cloned.1.call-start = ((), (), s32[]{:S(2)}) async-start(), calls=%async_computation.5 | async-start | bytes 6488064 | tf_op jit(solution)/shard_map/all_gather | solution.py:113
  109.3 142.2 %reduce-scatter.5.cloned.1.call-start = ((), (), s32[]{:S(2)}) async-start(), calls=%async_computation.6 | async-start | bytes 655360 | tf_op jit(solution)/shard_map/reduce_scatter | solution.py:117
  141.8 109.7 %copy-start.3 = (bf16[32,2048]{1,0:T(8,128)(2,1)S(1)}, bf16[32,2048]{1,0:T(8,128)(2,1)}, u32[]{:S(2)}) copy-start(bf16[32,2048]{1,0:T(8,128)(2,1)} %reduce-scatter.3.cloned.1.call-done) | copy-start | bytes 393220
Sparse Core Ops, SparseCore 0:
  9.5 44.3 all-gather.3
  55.9 49.4 all-gather.5
  108.8 20.2 reduce-scatter.2
  131.1 92.2 all-gather.7
  231.6 19.8 reduce-scatter.4
where the time goes:
time: 260 us
  waiting for transfers between devices  146 us (56%)
  blocking collectives  72.5 us (28%)
  matrix products  17.7 us (7%)
  between operations  13.3 us (5%)
  local copies, waits for them, and re-layouts  5.22 us (2%)
  other arithmetic  4.8 us (2%)
    all_gather x1, waiting for transfers between devices, local(): lax.all_gather(down_weight, 'sp', axis=0, tiled=True)  81.6 us
    all_gather x1, blocking collectives, local(): keys_one = lax.all_gather(key_first, 'sp', axis=0, tiled=True)  33.7 us
    all_gather x1, blocking collectives, local(): lax.all_gather(key_second, 'sp', axis=0, tiled=True)  32.2 us
    all_gather x1, waiting for transfers between devices, local(): lax.all_gather(out_weight, 'sp', axis=0, tiled=True)  22.5 us
    reduce_scatter x1, waiting for transfers between devices, local(): lax.psum_scatter(down_partial.astype(jnp.bfloat16), 'tp', scatter_dimensi...  20 us
    reduce_scatter x1, waiting for transfers between devices, local(): lax.psum_scatter(partial_value.astype(jnp.bfloat16), 'tp', scatter_dimens...  19.8 us
    dot_general x1, matrix products, local(): lax.dot_general(hidden, lax.all_gather(down_weight, 'sp', axis=0, tiled=T...  8 us
    all_gather x1, blocking collectives, local(): lax.all_gather((scaled_rows * norm_gain).astype(jnp.bfloat16), 'tp', axis...  6.59 us
  transfers between devices with their start and end apart: 5, of which 4 were waited for; matrix products, arithmetic and copies ran while one was open for 5% of the time, Pallas kernels for 0%

commit v1 on v0

v1 whole, which is shorter than its diff:
```python
import functools

import jax
import jax.numpy as jnp
from jax import lax
from jax.experimental import pallas as pl
from jax.experimental.pallas import tpu as pltpu
from jax.sharding import PartitionSpec as P

epsilon = 1e-06
ROWS_ROWS = (((1,), (1,)), ((), ()))


def split_sp(size):
    inner = 1
    while (2 * inner) * (2 * inner) <= size:
        inner *= 2
    return size // inner, inner


def kernel(
    Z,
    X,
    T,
    heads,
    residual,
    q_one,
    k_one,
    q_two,
    k_two,
    values,
    lam,
    head_gain,
    out_weight,
    norm_gain,
    gate_weight,
    up_weight,
    down_weight,
    result,
    kv,
    outw,
    downw,
    gate,
    up,
    attended,
    part,
    rec_one,
    after,
    normed,
    hidden,
    hidden_other,
    part_two,
    rec_two,
    local_sem,
    send_sem,
    recv_sem,
):
    f32, bf16 = jnp.float32, jnp.bfloat16
    s = lax.axis_index("sp")
    t = lax.axis_index("tp")
    z, x = s // X, s % X
    parity = z % 2
    zpair = z + 1 - 2 * parity
    spair = zpair * X + x
    tokens = q_one.shape[0]
    piece = tokens // T
    kw = k_one.shape[1]
    vw = values.shape[1]
    model = result.shape[1]
    group = X * down_weight.shape[0]

    def at_z(d):
        return (z + d) % Z

    def from_z(d):
        return (z - d + Z) % Z

    def at_x(d):
        return (x + d) % X

    def from_x(d):
        return (x - d + X) % X

    def at_t(d):
        return (t + d) % T

    def from_t(d):
        return (t - d + T) % T

    barrier = pltpu.get_barrier_semaphore()
    peers = [(at_z(d) * X + x, t) for d in range(1, Z)]
    peers += [(z * X + at_x(d), t) for d in range(1, X)]
    peers += [(s, at_t(d)) for d in range(1, T)]
    peers += [(spair, at_t(d)) for d in range(1, T)]
    for sp_at, tp_at in peers:
        pl.semaphore_signal(
            barrier, inc=1, device_id={"sp": sp_at, "tp": tp_at},
            device_id_type=pl.DeviceIdType.MESH,
        )

    locals_ = [
        pltpu.make_async_copy(k_one, kv.at[s, :, pl.ds(0, kw)], local_sem.at[0]),
        pltpu.make_async_copy(k_two, kv.at[s, :, pl.ds(kw, kw)], local_sem.at[1]),
        pltpu.make_async_copy(values, kv.at[s, :, pl.ds(2 * kw, vw)], local_sem.at[2]),
        pltpu.make_async_copy(out_weight, outw.at[s], local_sem.at[3]),
        pltpu.make_async_copy(down_weight, downw.at[z // 2, x], local_sem.at[4]),
        pltpu.make_async_copy(gate_weight, gate, local_sem.at[5]),
        pltpu.make_async_copy(up_weight, up, local_sem.at[6]),
    ]
    for copy in locals_:
        copy.start()

    names = {}
    sent = []

    def slot(name):
        return names.setdefault(name, len(names))

    def send(src, dst, name, sp_at, tp_at):
        k = slot(name)
        copy = pltpu.make_async_remote_copy(
            src_ref=src, dst_ref=dst, send_sem=send_sem.at[k], recv_sem=recv_sem.at[k],
            device_id={"sp": sp_at, "tp": tp_at}, device_id_type=pl.DeviceIdType.MESH,
        )
        copy.start()
        sent.append(copy)

    def arrive(ref, name):
        k = slot(name)
        pltpu.make_async_remote_copy(
            src_ref=ref, dst_ref=ref, send_sem=send_sem.at[k], recv_sem=recv_sem.at[k],
            device_id={"sp": s, "tp": t}, device_id_type=pl.DeviceIdType.MESH,
        ).wait_recv()

    def by_s(buffer):
        return lambda zz, xx: buffer.at[zz * X + xx]

    def down_at(zz, xx):
        return downw.at[zz // 2, xx]

    kv_at, out_at = by_s(kv), by_s(outw)

    def send_z(kind, ref, d):
        send(ref(z, x), ref(z, x), (kind, "z", d), at_z(d) * X + x, t)

    def wait_z(kind, ref, d):
        arrive(ref(from_z(d), x), (kind, "z", d))

    def forward_x(kind, ref, d):
        for dx in range(1, X):
            block = ref(from_z(d), x)
            send(block, block, (kind, "x", d, dx), z * X + at_x(dx), t)

    def wait_x(kind, ref, d):
        for dx in range(1, X):
            arrive(ref(from_z(d), from_x(dx)), (kind, "x", d, dx))

    for copy in locals_[:3]:
        copy.wait()
    pl.semaphore_wait(barrier, len(peers))
    for d in range(1, Z):
        send_z("kv", kv_at, d)
    forward_x("kv", kv_at, 0)
    locals_[3].wait()
    for d in range(1, Z):
        send_z("out", out_at, d)
    locals_[4].wait()
    for d in range(2, Z, 2):
        send_z("down", down_at, d)
    for d in range(1, Z):
        wait_z("kv", kv_at, d)
        forward_x("kv", kv_at, d)
    forward_x("out", out_at, 0)
    for d in range(Z):
        wait_x("kv", kv_at, d)

    head_size = q_one.shape[1] // heads
    value_size = vw // heads
    per = 128 // head_size
    scale = head_size ** (-0.5)
    source_count = kv.shape[0]
    block_count = max(1, (source_count * tokens) // 1024)
    block_sources = source_count // block_count
    block_keys = block_sources * tokens
    lanes = lax.broadcasted_iota(jnp.int32, (1, per * head_size), 1) // head_size

    def map_outputs(q_ref, base, first):
        width = per * head_size
        q = q_ref[:, first * head_size : first * head_size + width]
        stacked = jnp.concatenate(
            [jnp.where(lanes == i, q, jnp.zeros_like(q)) for i in range(per)], axis=0
        )

        def block(b, state):
            rows = pl.ds(b * block_sources, block_sources)
            keys = kv[rows, :, base + first * head_size : base + first * head_size + width]
            scores = lax.dot_general(
                stacked, keys.reshape(block_keys, width), ROWS_ROWS, preferred_element_type=f32
            ) * scale
            newest = jnp.max(scores, axis=1, keepdims=True)
            if state is not None:
                newest = jnp.maximum(newest, state[0])
            shifted = jnp.exp(scores - newest)
            totals = jnp.sum(shifted, axis=1, keepdims=True)
            rounded = shifted.astype(bf16)
            products = []
            for i in range(per):
                start = 2 * kw + (first + i) * value_size
                v = kv[rows, :, start : start + value_size].reshape(block_keys, value_size)
                products.append(
                    jnp.dot(
                        rounded[i * tokens : (i + 1) * tokens], v, preferred_element_type=f32
                    )
                )
            product = jnp.concatenate(products, axis=0)
            if state is not None:
                factor = jnp.exp(state[0] - newest)
                totals = totals + state[1] * factor
                product = product + state[2] * factor
            return newest, totals, product

        if block_count == 1:
            state = block(0, None)
        else:
            state = lax.fori_loop(
                0,
                block_count,
                block,
                (
                    jnp.full((per * tokens, 1), -jnp.inf, f32),
                    jnp.zeros((per * tokens, 1), f32),
                    jnp.zeros((per * tokens, value_size), f32),
                ),
            )
        return state[2] / state[1]

    for first in range(0, heads, per):
        one = map_outputs(q_one, 0, first)
        two = map_outputs(q_two, kw, first)
        for i in range(per):
            rows = slice(i * tokens, (i + 1) * tokens)
            difference = one[rows] - lam[first + i] * two[rows]
            scaled = difference * lax.rsqrt(
                jnp.mean(difference * difference, axis=1, keepdims=True) + epsilon
            )
            start = (first + i) * value_size
            attended[:, start : start + value_size] = (scaled * head_gain[...]).astype(bf16)

    for d in range(1, Z):
        wait_z("out", out_at, d)
        forward_x("out", out_at, d)
    forward_x("down", down_at, 0)
    for d in range(Z):
        wait_x("out", out_at, d)

    rows_out = out_weight.shape[0]
    chunk = min(512, model)
    for c in range(0, model, chunk):
        cols = slice(c, c + chunk)
        weight = outw[c // rows_out : (c + chunk) // rows_out].reshape(chunk, vw)
        product = lax.dot_general(
            attended[...], weight, ROWS_ROWS, preferred_element_type=f32
        ).astype(bf16)
        part[:, :, cols] = product.reshape(T, piece, chunk)
        for d in range(1, T):
            send(
                part.at[at_t(d), :, pl.ds(c, chunk)],
                rec_one.at[t, :, pl.ds(c, chunk)],
                ("one", c, d), s, at_t(d),
            )
    rec_one[t] = part[t]
    for c in range(0, model, chunk):
        for d in range(1, T):
            arrive(rec_one.at[from_t(d), :, pl.ds(c, chunk)], ("one", c, d))
    summed = rec_one[0].astype(f32)
    for i in range(1, T):
        summed = summed + rec_one[i].astype(f32)
    stream = (residual[...].astype(f32) + summed).astype(bf16).astype(f32)
    after[...] = stream
    scaled = stream * lax.rsqrt(jnp.mean(stream * stream, axis=1, keepdims=True) + epsilon)
    normed[t] = (scaled * norm_gain[...]).astype(bf16)
    for d in range(1, T):
        send(normed.at[t], normed.at[t], ("norm", d), s, at_t(d))
    locals_[5].wait()
    locals_[6].wait()
    for d in range(1, T):
        arrive(normed.at[from_t(d)], ("norm", d))

    width = hidden.shape[1]
    spans = [(c, min(512, width - c)) for c in range(0, width, 512)]
    rows_in = normed[...].reshape(tokens, model)
    for c, n in spans:
        gate_part = jnp.dot(rows_in, gate[:, c : c + n], preferred_element_type=f32)
        up_part = jnp.dot(rows_in, up[:, c : c + n], preferred_element_type=f32)
        hidden[:, c : c + n] = (gate_part / (1.0 + jnp.exp(-gate_part)) * up_part).astype(bf16)
        send(
            hidden.at[:, pl.ds(c, n)], hidden_other.at[:, pl.ds(c, n)], ("hid", c), spair, t
        )
    for d in range(2, Z, 2):
        wait_z("down", down_at, d)
        forward_x("down", down_at, d)
    for d in range(0, Z, 2):
        wait_x("down", down_at, d)

    def project(which, source, sp_at, first_step):
        for g in range(Z // 2):
            cols = slice(g * group, (g + 1) * group)
            product = lax.dot_general(
                source[...], downw[g].reshape(group, width), ROWS_ROWS,
                preferred_element_type=f32,
            ).astype(bf16)
            part_two[which, :, :, cols] = product.reshape(T, piece, group)
            for d in range(first_step, T):
                send(
                    part_two.at[which, at_t(d), :, pl.ds(g * group, group)],
                    rec_two.at[parity, t, :, pl.ds(g * group, group)],
                    ("two", which, g, d), sp_at, at_t(d),
                )

    for c, n in spans:
        arrive(hidden_other.at[:, pl.ds(c, n)], ("hid", c))
    project(1, hidden_other, spair, 0)
    project(0, hidden, s, 1)
    rec_two[parity, t] = part_two[0, t]
    for g in range(Z // 2):
        for d in range(1, T):
            arrive(
                rec_two.at[parity, from_t(d), :, pl.ds(g * group, group)], ("two", 0, g, d)
            )
        for d in range(T):
            arrive(
                rec_two.at[1 - parity, from_t(d), :, pl.ds(g * group, group)], ("two", 1, g, d)
            )
    for side in range(2):
        for g in range(Z // 2):
            start = (2 * g + side) * group
            total = rec_two[side, 0, :, g * group : (g + 1) * group].astype(f32)
            for i in range(1, T):
                total = total + rec_two[side, i, :, g * group : (g + 1) * group].astype(f32)
            result[:, start : start + group] = (
                after[:, start : start + group] + total
            ).astype(bf16)
    for copy in sent:
        copy.wait_send()


def local(Z, X, T, *arrays):
    (residual, q_one, k_one, q_two, k_two, values, lam, head_gain, out_weight, norm_gain,
     gate_weight, up_weight, down_weight) = arrays
    sp = Z * X
    bf16 = jnp.bfloat16
    tokens, kw = k_one.shape
    vw = values.shape[1]
    piece, model = residual.shape
    width = gate_weight.shape[1]
    rows_down = down_weight.shape[0]
    half = model // 2
    vmem = pl.BlockSpec(memory_space=pltpu.VMEM)
    anywhere = pl.BlockSpec(memory_space=pl.ANY)
    smem = pl.BlockSpec(memory_space=pltpu.SMEM)
    semaphores = 2 * (Z + Z * X) + Z + Z * X + 64
    return pl.pallas_call(
        functools.partial(kernel, Z, X, T, lam.shape[0]),
        out_shape=jax.ShapeDtypeStruct((piece, model), bf16),
        in_specs=[
            vmem, vmem, anywhere, vmem, anywhere, anywhere, smem, vmem, anywhere, vmem,
            anywhere, anywhere, anywhere,
        ],
        out_specs=vmem,
        scratch_shapes=[
            pltpu.VMEM((sp, tokens, 2 * kw + vw), bf16),
            pltpu.VMEM((sp, out_weight.shape[0], vw), bf16),
            pltpu.VMEM((Z // 2, X, rows_down, width), bf16),
            pltpu.VMEM(gate_weight.shape, bf16),
            pltpu.VMEM(up_weight.shape, bf16),
            pltpu.VMEM((tokens, vw), bf16),
            pltpu.VMEM((T, piece, model), bf16),
            pltpu.VMEM((T, piece, model), bf16),
            pltpu.VMEM((piece, model), jnp.float32),
            pltpu.VMEM((T, piece, model), bf16),
            pltpu.VMEM((tokens, width), bf16),
            pltpu.VMEM((tokens, width), bf16),
            pltpu.VMEM((2, T, piece, half), bf16),
            pltpu.VMEM((2, T, piece, half), bf16),
            pltpu.SemaphoreType.DMA((7,)),
            pltpu.SemaphoreType.DMA((semaphores,)),
            pltpu.SemaphoreType.DMA((semaphores,)),
        ],
        compiler_params=pltpu.CompilerParams(
            collective_id=0, has_side_effects=True, vmem_limit_bytes=60 * 1024 * 1024
        ),
    )(
        residual, q_one, k_one, q_two, k_two, values, lam, head_gain.reshape(1, -1), out_weight,
        norm_gain.reshape(1, -1), gate_weight, up_weight, down_weight,
    )


def solution(mesh):
    Z, X = split_sp(mesh.shape["sp"])
    return jax.shard_map(
        functools.partial(local, Z, X, mesh.shape["tp"]),
        mesh=mesh,
        in_specs=(
            P(("sp", "tp"), None),
            P("sp", "tp"),
            P("sp", "tp"),
            P("sp", "tp"),
            P("sp", "tp"),
            P("sp", "tp"),
            P("tp"),
            P(),
            P("sp", "tp"),
            P(),
            P(None, "tp"),
            P(None, "tp"),
            P("sp", "tp"),
        ),
        out_specs=P(("sp", "tp"), None),
        check_vma=False,
    )
```

time: 260 us -> 128 us (0.49)
  the two profiles are of different devices: /device:TPU:0 before, /device:TPU:17 now
where the time goes in v1:
time: 128 us
  Pallas kernels  127 us (99%)
  local copies, waits for them, and re-layouts  1.57 us (1%)
    pallas_call x1, Pallas kernels, local(): pl.pallas_call(functools.partial(kernel, Z, X, T, lam.shape[0]), out_shap...  127 us

profile of v1, /device:TPU:17, one launch (start us, length us, event | category | flops | bytes accessed | tf_op | source)
XLA Modules:
  0.0 128.2 jit_solution(2927546980952089661)
XLA Ops:
  0.0 126.6 %shard_map.127 = bf16[32,2048]{1,0:T(8,128)(2,1)} custom-call(bf16[32,2048]{1,0:T(8,128)(2,1)} %residual.1, bf16[128,256]{1,0:T(8,128)(2,1)} %q_one.1, bf16[128,256]{1,0:T(8,128)(2,1)} %k_one.1, bf16[128,256]{1,0:T(8,128)(2,1)} %q_two.1, bf16[128,256]{1,0:T(8,128)(2,1)} %k_two.1, bf16[128,512]{1,0:T(8,128)(2,1)} %values.1, f32[4]{0:T(128)} %lam.1, ...), custom_call_target="tpu_custom_call" | custom-call | tf_op jit(solution)/shard_map/pallas_call | solution.py:362
  126.6 1.6 %copy.15 = bf16[32,2048]{1,0:T(8,128)(2,1)} copy(bf16[32,2048]{1,0:T(8,128)(2,1)} %shard_map.127) | data formatting | bytes 262144

commit v2 on v1

v2 whole, which is shorter than its diff:
```python
import functools

import jax
import jax.numpy as jnp
from jax import lax
from jax.experimental import pallas as pl
from jax.experimental.pallas import tpu as pltpu
from jax.sharding import PartitionSpec as P

epsilon = 1e-06
ROWS_ROWS = (((1,), (1,)), ((), ()))


def split_sp(size):
    inner = 1
    while (2 * inner) * (2 * inner) <= size:
        inner *= 2
    return size // inner, inner


def kernel(
    Z,
    X,
    T,
    C,
    heads,
    residual,
    q_one,
    k_one,
    q_two,
    k_two,
    values,
    lam,
    head_gain,
    out_weight,
    norm_gain,
    gate_weight,
    up_weight,
    down_weight,
    result,
    queries,
    queries_out,
    kv,
    kv_out,
    outw,
    downw,
    gate,
    up,
    attended,
    part_one,
    rec_one,
    after,
    normed,
    hidden,
    part_two,
    rec_two,
    local_sem,
    send_sem,
    recv_sem,
):
    f32, bf16 = jnp.float32, jnp.bfloat16
    s = lax.axis_index("sp")
    t = lax.axis_index("tp")
    z, x = s // X, s % X
    parity = z % 2
    other = 1 - parity
    zpair = z + 1 - 2 * parity
    spair = zpair * X + x
    tokens = q_one.shape[0]
    piece = tokens // T
    kw = k_one.shape[1] // 2
    vw = values.shape[1] // 2
    group = X * down_weight.shape[0]
    groups = Z // 2

    def at_z(d):
        return (z + d) % Z

    def from_z(d):
        return (z - d + Z) % Z

    def at_x(d):
        return (x + d) % X

    def from_x(d):
        return (x - d + X) % X

    def at_t(d):
        return (t + d) % T

    def from_t(d):
        return (t - d + T) % T

    barrier = pltpu.get_barrier_semaphore()
    peers = [(at_z(d) * X + x, t) for d in range(1, Z)]
    peers += [(z * X + at_x(d), t) for d in range(1, X)]
    peers += [(s, at_t(d)) for d in range(1, T)]
    peers += [(spair, at_t(d)) for d in range(1, T)]
    for sp_at, tp_at in peers:
        pl.semaphore_signal(
            barrier, inc=1, device_id={"sp": sp_at, "tp": tp_at},
            device_id_type=pl.DeviceIdType.MESH,
        )

    def columns(ref, half, size):
        return ref.at[:, pl.ds(pl.multiple_of(half * size, size), size)]

    moves = [
        (columns(q_one, other, kw), queries_out.at[0]),
        (columns(q_two, other, kw), queries_out.at[1]),
        (columns(k_one, other, kw), kv_out.at[:, pl.ds(0, kw)]),
        (columns(k_two, other, kw), kv_out.at[:, pl.ds(kw, kw)]),
        (columns(values, other, vw), kv_out.at[:, pl.ds(2 * kw, vw)]),
        (columns(k_one, parity, kw), kv.at[s, :, pl.ds(0, kw)]),
        (columns(k_two, parity, kw), kv.at[s, :, pl.ds(kw, kw)]),
        (columns(values, parity, vw), kv.at[s, :, pl.ds(2 * kw, vw)]),
        (columns(q_one, parity, kw), queries.at[0, 0]),
        (columns(q_two, parity, kw), queries.at[0, 1]),
        (out_weight, outw.at[z // 2, x]),
        (down_weight, downw.at[z // 2, x]),
        (gate_weight, gate),
        (up_weight, up),
    ]
    moving = [
        pltpu.make_async_copy(src, dst, local_sem.at[i]) for i, (src, dst) in enumerate(moves)
    ]
    for copy in moving:
        copy.start()

    names = {}
    sent = []

    def slot(name):
        return names.setdefault(name, len(names))

    def send(src, dst, name, sp_at, tp_at):
        k = slot(name)
        copy = pltpu.make_async_remote_copy(
            src_ref=src, dst_ref=dst, send_sem=send_sem.at[k], recv_sem=recv_sem.at[k],
            device_id={"sp": sp_at, "tp": tp_at}, device_id_type=pl.DeviceIdType.MESH,
        )
        copy.start()
        sent.append(copy)

    def arrive(ref, name):
        k = slot(name)
        pltpu.make_async_remote_copy(
            src_ref=ref, dst_ref=ref, send_sem=send_sem.at[k], recv_sem=recv_sem.at[k],
            device_id={"sp": s, "tp": t}, device_id_type=pl.DeviceIdType.MESH,
        ).wait_recv()

    def kv_at(zz, xx):
        return kv.at[zz * X + xx]

    def out_at(zz, xx):
        return outw.at[zz // 2, xx]

    rows_chunk = down_weight.shape[0] // C

    def down_at(c):
        return lambda zz, xx: downw.at[zz // 2, xx, pl.ds(c * rows_chunk, rows_chunk)]

    def send_z(kind, ref, d):
        send(ref(z, x), ref(z, x), (kind, "z", d), at_z(d) * X + x, t)

    def wait_z(kind, ref, d):
        arrive(ref(from_z(d), x), (kind, "z", d))

    def forward_x(kind, ref, d):
        for dx in range(1, X):
            block = ref(from_z(d), x)
            send(block, block, (kind, "x", d, dx), z * X + at_x(dx), t)

    def wait_x(kind, ref, d):
        for dx in range(1, X):
            arrive(ref(from_z(d), from_x(dx)), (kind, "x", d, dx))

    def down_z(c):
        for d in range(2, Z, 2):
            send_z("down%d" % c, down_at(c), d)

    def down_own(c):
        forward_x("down%d" % c, down_at(c), 0)

    def down_forward(c):
        for d in range(2, Z, 2):
            wait_z("down%d" % c, down_at(c), d)
            forward_x("down%d" % c, down_at(c), d)

    for copy in moving[:8]:
        copy.wait()
    pl.semaphore_wait(barrier, len(peers))
    for d in range(1, Z):
        send(
            kv_out if d % 2 else kv.at[s], kv.at[s], ("kv", "z", d), at_z(d) * X + x, t
        )
        if d == 1:
            forward_x("kv", kv_at, 0)
            send(queries_out, queries.at[1], ("query",), spair, t)
    for copy in moving[8:12]:
        copy.wait()
    for d in range(2, Z, 2):
        send_z("out", out_at, d)
    down_z(0)
    for d in range(1, Z):
        wait_z("kv", kv_at, d)
        forward_x("kv", kv_at, d)
    forward_x("out", out_at, 0)
    down_own(0)
    arrive(queries.at[1], ("query",))
    for d in range(Z):
        wait_x("kv", kv_at, d)

    half_heads = heads // 2
    head_size = kw // half_heads
    value_size = vw // half_heads
    per = min(half_heads, 128 // head_size)
    scale = head_size ** (-0.5)
    source_count = kv.shape[0]
    block_count = max(1, (source_count * tokens) // 1024)
    block_sources = source_count // block_count
    block_keys = block_sources * tokens
    lanes = lax.broadcasted_iota(jnp.int32, (1, per * head_size), 1) // head_size

    def map_outputs(which, index, first):
        width = per * head_size
        q = queries[which, index, :, first * head_size : first * head_size + width]
        stacked = jnp.concatenate(
            [jnp.where(lanes == i, q, jnp.zeros_like(q)) for i in range(per)], axis=0
        )
        base = index * kw + first * head_size

        def block(b, state):
            rows = pl.ds(b * block_sources, block_sources)
            keys = kv[rows, :, base : base + width]
            scores = lax.dot_general(
                stacked, keys.reshape(block_keys, width), ROWS_ROWS, preferred_element_type=f32
            ) * scale
            newest = jnp.max(scores, axis=1, keepdims=True)
            if state is not None:
                newest = jnp.maximum(newest, state[0])
            shifted = jnp.exp(scores - newest)
            totals = jnp.sum(shifted, axis=1, keepdims=True)
            rounded = shifted.astype(bf16)
            products = []
            for i in range(per):
                start = 2 * kw + (first + i) * value_size
                v = kv[rows, :, start : start + value_size].reshape(block_keys, value_size)
                products.append(
                    jnp.dot(
                        rounded[i * tokens : (i + 1) * tokens], v, preferred_element_type=f32
                    )
                )
            product = jnp.concatenate(products, axis=0)
            if state is not None:
                factor = jnp.exp(state[0] - newest)
                totals = totals + state[1] * factor
                product = product + state[2] * factor
            return newest, totals, product

        if block_count == 1:
            state = block(0, None)
        else:
            state = lax.fori_loop(
                0,
                block_count,
                block,
                (
                    jnp.full((per * tokens, 1), -jnp.inf, f32),
                    jnp.zeros((per * tokens, 1), f32),
                    jnp.zeros((per * tokens, value_size), f32),
                ),
            )
        return state[2] / state[1]

    for which in (1, 0):
        for first in range(0, half_heads, per):
            one = map_outputs(which, 0, first)
            two = map_outputs(which, 1, first)
            for i in range(per):
                rows = slice(i * tokens, (i + 1) * tokens)
                difference = one[rows] - lam[parity * half_heads + first + i] * two[rows]
                scaled = difference * lax.rsqrt(
                    jnp.mean(difference * difference, axis=1, keepdims=True) + epsilon
                )
                start = (first + i) * value_size
                attended[which, parity, :, start : start + value_size] = (
                    scaled * head_gain[...]
                ).astype(bf16)
        send(
            attended.at[which, parity], attended.at[1 - which, parity], ("att", which), spair, t
        )

    for d in range(2, Z, 2):
        wait_z("out", out_at, d)
        forward_x("out", out_at, d)
    for c in range(1, C):
        if c == 1:
            down_z(c)
        down_own(c)
    for d in range(0, Z, 2):
        wait_x("out", out_at, d)
    for which in (1, 0):
        arrive(attended.at[1 - which, other], ("att", which))

    def spread(kind, which, g, product, part, rec):
        cols = slice(g * group, (g + 1) * group)
        part[which, :, :, cols] = product.astype(bf16).reshape(T, piece, group)
        for d in range(0 if which else 1, T):
            send(
                part.at[which, at_t(d), :, pl.ds(g * group, group)],
                rec.at[parity, t, :, pl.ds(g * group, group)],
                (kind, which, g, d), spair if which else s, at_t(d),
            )

    def collect(kind, base, part, rec, put):
        rec[parity, t] = part[0, t]
        for g in range(groups):
            for d in range(1, T):
                arrive(
                    rec.at[parity, from_t(d), :, pl.ds(g * group, group)], (kind, 0, g, d)
                )
            for d in range(T):
                arrive(
                    rec.at[1 - parity, from_t(d), :, pl.ds(g * group, group)], (kind, 1, g, d)
                )
            for side in range(2):
                start = (2 * g + side) * group
                total = rec[side, 0, :, g * group : (g + 1) * group].astype(f32)
                for i in range(1, T):
                    total = total + rec[side, i, :, g * group : (g + 1) * group].astype(f32)
                put(start, base[:, start : start + group].astype(f32) + total)

    for g in range(groups):
        weight = outw[g].reshape(group, 2 * vw)
        both = [attended[:, h].reshape(2 * tokens, vw) for h in range(2)]
        product = lax.dot_general(
            both[0], weight[:, :vw], ROWS_ROWS, preferred_element_type=f32
        ) + lax.dot_general(both[1], weight[:, vw:], ROWS_ROWS, preferred_element_type=f32)
        for which in (1, 0):
            spread(
                "one", which, g, product[which * tokens : (which + 1) * tokens], part_one, rec_one
            )
    if C > 2:
        down_z(2)
    down_forward(0)

    def put_after(start, block):
        after[:, start : start + group] = block.astype(bf16).astype(f32)

    collect("one", residual, part_one, rec_one, put_after)
    stream = after[...]
    scaled = stream * lax.rsqrt(jnp.mean(stream * stream, axis=1, keepdims=True) + epsilon)
    normed[t] = (scaled * norm_gain[...]).astype(bf16)
    for d in range(1, T):
        send(normed.at[t], normed.at[t], ("norm", d), s, at_t(d))
    for c in range(3, C):
        down_z(c)
    if C > 1:
        down_forward(1)
    for copy in moving[12:]:
        copy.wait()
    for d in range(1, T):
        arrive(normed.at[from_t(d)], ("norm", d))

    width = hidden.shape[2]
    spans = [(c, min(512, width - c)) for c in range(0, width, 512)]
    rows_in = normed[...].reshape(tokens, normed.shape[2])
    for c, n in spans:
        gate_part = jnp.dot(rows_in, gate[:, c : c + n], preferred_element_type=f32)
        up_part = jnp.dot(rows_in, up[:, c : c + n], preferred_element_type=f32)
        hidden[0, :, c : c + n] = (
            gate_part / (1.0 + jnp.exp(-gate_part)) * up_part
        ).astype(bf16)
        send(hidden.at[0, :, pl.ds(c, n)], hidden.at[1, :, pl.ds(c, n)], ("hid", c), spair, t)
    for c in range(2, C):
        down_forward(c)
    for c in range(C):
        for d in range(0, Z, 2):
            wait_x("down%d" % c, down_at(c), d)
    for which in range(2):
        if which:
            for c, n in spans:
                arrive(hidden.at[1, :, pl.ds(c, n)], ("hid", c))
        for g in range(groups):
            product = lax.dot_general(
                hidden[which], downw[g].reshape(group, width), ROWS_ROWS,
                preferred_element_type=f32,
            )
            spread("two", which, g, product, part_two, rec_two)

    def put_result(start, block):
        result[:, start : start + group] = block.astype(bf16)

    collect("two", after, part_two, rec_two, put_result)
    for copy in sent:
        copy.wait_send()


def local(Z, X, T, *arrays):
    (residual, q_one, k_one, q_two, k_two, values, lam, head_gain, out_weight, norm_gain,
     gate_weight, up_weight, down_weight) = arrays
    sp = Z * X
    bf16 = jnp.bfloat16
    tokens, kw = k_one.shape
    vw = values.shape[1]
    piece, model = residual.shape
    width = gate_weight.shape[1]
    rows_down = down_weight.shape[0]
    C = max(1, min(4, rows_down // 32))
    half = model // 2
    vmem = pl.BlockSpec(memory_space=pltpu.VMEM)
    anywhere = pl.BlockSpec(memory_space=pl.ANY)
    smem = pl.BlockSpec(memory_space=pltpu.SMEM)
    semaphores = Z + Z * X + (1 + C) * (Z // 2) * (1 + X) + 8 * T * Z + 64
    return pl.pallas_call(
        functools.partial(kernel, Z, X, T, C, lam.shape[0]),
        out_shape=jax.ShapeDtypeStruct((piece, model), bf16),
        in_specs=[
            vmem, anywhere, anywhere, anywhere, anywhere, anywhere, smem, vmem, anywhere, vmem,
            anywhere, anywhere, anywhere,
        ],
        out_specs=vmem,
        scratch_shapes=[
            pltpu.VMEM((2, 2, tokens, kw // 2), bf16),
            pltpu.VMEM((2, tokens, kw // 2), bf16),
            pltpu.VMEM((sp, tokens, kw + vw // 2), bf16),
            pltpu.VMEM((tokens, kw + vw // 2), bf16),
            pltpu.VMEM((Z // 2, X, out_weight.shape[0], vw), bf16),
            pltpu.VMEM((Z // 2, X, rows_down, width), bf16),
            pltpu.VMEM(gate_weight.shape, bf16),
            pltpu.VMEM(up_weight.shape, bf16),
            pltpu.VMEM((2, 2, tokens, vw // 2), bf16),
            pltpu.VMEM((2, T, piece, half), bf16),
            pltpu.VMEM((2, T, piece, half), bf16),
            pltpu.VMEM((piece, model), jnp.float32),
            pltpu.VMEM((T, piece, model), bf16),
            pltpu.VMEM((2, tokens, width), bf16),
            pltpu.VMEM((2, T, piece, half), bf16),
            pltpu.VMEM((2, T, piece, half), bf16),
            pltpu.SemaphoreType.DMA((14,)),
            pltpu.SemaphoreType.DMA((semaphores,)),
            pltpu.SemaphoreType.DMA((semaphores,)),
        ],
        compiler_params=pltpu.CompilerParams(
            collective_id=0, has_side_effects=True, vmem_limit_bytes=60 * 1024 * 1024
        ),
    )(
        residual, q_one, k_one, q_two, k_two, values, lam, head_gain.reshape(1, -1), out_weight,
        norm_gain.reshape(1, -1), gate_weight, up_weight, down_weight,
    )


def solution(mesh):
    Z, X = split_sp(mesh.shape["sp"])
    return jax.shard_map(
        functools.partial(local, Z, X, mesh.shape["tp"]),
        mesh=mesh,
        in_specs=(
            P(("sp", "tp"), None),
            P("sp", "tp"),
            P("sp", "tp"),
            P("sp", "tp"),
            P("sp", "tp"),
            P("sp", "tp"),
            P("tp"),
            P(),
            P("sp", "tp"),
            P(),
            P(None, "tp"),
            P(None, "tp"),
            P("sp", "tp"),
        ),
        out_specs=P(("sp", "tp"), None),
        check_vma=False,
    )
```

time: 128 us -> 90.8 us (0.71)
  the two profiles are of different devices: /device:TPU:17 before, /device:TPU:0 now
where the time goes in v2:
time: 90.8 us; the launch traced here: 90.7 us
  Pallas kernels  89.1 us (98%)
  local copies, waits for them, and re-layouts  1.57 us (2%)
    pallas_call x1, Pallas kernels, local(): pl.pallas_call(functools.partial(kernel, Z, X, T, C, lam.shape[0]), out_s...  89.1 us

profile of v2, /device:TPU:0, one launch (start us, length us, event | category | flops | bytes accessed | tf_op | source)
XLA Modules:
  0.0 90.7 jit_solution(6983680779874277015)
XLA Ops:
  0.0 89.1 %shard_map.127 = bf16[32,2048]{1,0:T(8,128)(2,1)} custom-call(bf16[32,2048]{1,0:T(8,128)(2,1)} %residual.1, bf16[128,256]{1,0:T(8,128)(2,1)} %q_one.1, bf16[128,256]{1,0:T(8,128)(2,1)} %k_one.1, bf16[128,256]{1,0:T(8,128)(2,1)} %q_two.1, bf16[128,256]{1,0:T(8,128)(2,1)} %k_two.1, bf16[128,512]{1,0:T(8,128)(2,1)} %values.1, f32[4]{0:T(128)} %lam.1, ...), custom_call_target="tpu_custom_call" | custom-call | tf_op jit(solution)/shard_map/pallas_call | solution.py:416
  89.1 1.6 %copy.15 = bf16[32,2048]{1,0:T(8,128)(2,1)} copy(bf16[32,2048]{1,0:T(8,128)(2,1)} %shard_map.127) | data formatting | bytes 262144

commit v3 on v2

--- a/solution.py
+++ b/solution.py
@@ -9,6 +9,9 @@
 
 epsilon = 1e-06
 ROWS_ROWS = (((1,), (1,)), ((), ()))
+CHUNKS = 8
+STARTS = (0, 3, 6, 8)
+FORWARDS = (2, 4, 8)
 
 
 def split_sp(size):
@@ -149,8 +152,13 @@
             device_id={"sp": s, "tp": t}, device_id_type=pl.DeviceIdType.MESH,
         ).wait_recv()
 
-    def kv_at(zz, xx):
-        return kv.at[zz * X + xx]
+    def kv_at(lo, hi):
+        return lambda zz, xx: kv.at[zz * X + xx, :, pl.ds(lo, hi - lo)]
+
+    parts = [
+        (kind, kv_at(lo, hi), lo, hi)
+        for kind, lo, hi in (("kvk", 0, 2 * kw), ("kvv", 2 * kw, 2 * kw + vw))
+    ]
 
     def out_at(zz, xx):
         return outw.at[zz // 2, xx]
@@ -190,26 +198,33 @@
     for copy in moving[:8]:
         copy.wait()
     pl.semaphore_wait(barrier, len(peers))
-    for d in range(1, Z):
-        send(
-            kv_out if d % 2 else kv.at[s], kv.at[s], ("kv", "z", d), at_z(d) * X + x, t
-        )
-        if d == 1:
-            forward_x("kv", kv_at, 0)
+    for kind, ref, lo, hi in parts:
+        cols = pl.ds(lo, hi - lo)
+        for d in range(1, Z):
+            source = kv_out.at[:, cols] if d % 2 else kv.at[s, :, cols]
+            send(source, kv.at[s, :, cols], (kind, "z", d), at_z(d) * X + x, t)
+        forward_x(kind, ref, 0)
+        if lo == 0:
             send(queries_out, queries.at[1], ("query",), spair, t)
     for copy in moving[8:12]:
         copy.wait()
     for d in range(2, Z, 2):
         send_z("out", out_at, d)
-    down_z(0)
-    for d in range(1, Z):
-        wait_z("kv", kv_at, d)
-        forward_x("kv", kv_at, d)
+    starts = [min(C, k * C // CHUNKS) for k in STARTS]
+    forwards = [min(C, k * C // CHUNKS) for k in FORWARDS]
+    for c in range(starts[0]):
+        down_z(c)
+    for kind, ref, lo, hi in parts:
+        for d in range(1, Z):
+            wait_z(kind, ref, d)
+            forward_x(kind, ref, d)
     forward_x("out", out_at, 0)
-    down_own(0)
+    for c in range(starts[0]):
+        down_own(c)
     arrive(queries.at[1], ("query",))
-    for d in range(Z):
-        wait_x("kv", kv_at, d)
+    for kind, ref, lo, hi in parts:
+        for d in range(Z):
+            wait_x(kind, ref, d)
 
     half_heads = heads // 2
     head_size = kw // half_heads
@@ -294,9 +309,9 @@
     for d in range(2, Z, 2):
         wait_z("out", out_at, d)
         forward_x("out", out_at, d)
-    for c in range(1, C):
-        if c == 1:
-            down_z(c)
+    for c in range(starts[0], starts[1]):
+        down_z(c)
+    for c in range(starts[0], C):
         down_own(c)
     for d in range(0, Z, 2):
         wait_x("out", out_at, d)
@@ -341,9 +356,10 @@
             spread(
                 "one", which, g, product[which * tokens : (which + 1) * tokens], part_one, rec_one
             )
-    if C > 2:
-        down_z(2)
-    down_forward(0)
+    for c in range(starts[1], starts[2]):
+        down_z(c)
+    for c in range(forwards[0]):
+        down_forward(c)
 
     def put_after(start, block):
         after[:, start : start + group] = block.astype(bf16).astype(f32)
@@ -354,10 +370,10 @@
     normed[t] = (scaled * norm_gain[...]).astype(bf16)
     for d in range(1, T):
         send(normed.at[t], normed.at[t], ("norm", d), s, at_t(d))
-    for c in range(3, C):
+    for c in range(starts[2], C):
         down_z(c)
-    if C > 1:
-        down_forward(1)
+    for c in range(forwards[0], forwards[1]):
+        down_forward(c)
     for copy in moving[12:]:
         copy.wait()
     for d in range(1, T):
@@ -373,7 +389,7 @@
             gate_part / (1.0 + jnp.exp(-gate_part)) * up_part
         ).astype(bf16)
         send(hidden.at[0, :, pl.ds(c, n)], hidden.at[1, :, pl.ds(c, n)], ("hid", c), spair, t)
-    for c in range(2, C):
+    for c in range(forwards[1], C):
         down_forward(c)
     for c in range(C):
         for d in range(0, Z, 2):
@@ -407,12 +423,12 @@
     piece, model = residual.shape
     width = gate_weight.shape[1]
     rows_down = down_weight.shape[0]
-    C = max(1, min(4, rows_down // 32))
+    C = max(1, min(CHUNKS, rows_down // 32))
     half = model // 2
     vmem = pl.BlockSpec(memory_space=pltpu.VMEM)
     anywhere = pl.BlockSpec(memory_space=pl.ANY)
     smem = pl.BlockSpec(memory_space=pltpu.SMEM)
-    semaphores = Z + Z * X + (1 + C) * (Z // 2) * (1 + X) + 8 * T * Z + 64
+    semaphores = 2 * (Z + Z * X) + (1 + C) * (Z // 2) * (1 + X) + 8 * T * Z + 64
     return pl.pallas_call(
         functools.partial(kernel, Z, X, T, C, lam.shape[0]),
         out_shape=jax.ShapeDtypeStruct((piece, model), bf16),

time: 90.8 us -> 86.2 us (0.949)
  Pallas kernels: 89.1 us -> 84.5 us
    pallas_call x1, Pallas kernels: 89.1 us -> 84.5 us  [local(): pl.pallas_call(functools.partial(kernel, Z, X, T, C, lam.shape[0]), out_s...]
where the time goes in v3:
time: 86.2 us; the launch traced here: 86 us
  Pallas kernels  84.5 us (98%)
  local copies, waits for them, and re-layouts  1.57 us (2%)
    pallas_call x1, Pallas kernels, local(): pl.pallas_call(functools.partial(kernel, Z, X, T, C, lam.shape[0]), out_s...  84.5 us

profile of v3, /device:TPU:0, one launch (start us, length us, event | category | flops | bytes accessed | tf_op | source)
XLA Modules:
  0.0 86.0 jit_solution(4593002680267920609)
XLA Ops:
  0.0 84.5 %shard_map.127 = bf16[32,2048]{1,0:T(8,128)(2,1)} custom-call(bf16[32,2048]{1,0:T(8,128)(2,1)} %residual.1, bf16[128,256]{1,0:T(8,128)(2,1)} %q_one.1, bf16[128,256]{1,0:T(8,128)(2,1)} %k_one.1, bf16[128,256]{1,0:T(8,128)(2,1)} %q_two.1, bf16[128,256]{1,0:T(8,128)(2,1)} %k_two.1, bf16[128,512]{1,0:T(8,128)(2,1)} %values.1, f32[4]{0:T(128)} %lam.1, ...), custom_call_target="tpu_custom_call" | custom-call | tf_op jit(solution)/shard_map/pallas_call | solution.py:432
  84.5 1.6 %copy.15 = bf16[32,2048]{1,0:T(8,128)(2,1)} copy(bf16[32,2048]{1,0:T(8,128)(2,1)} %shard_map.127) | data formatting | bytes 262144
